TPU v7x, 32 devices: a whole 2x2x4 slice. The times are simulated.
32 devices in a mesh: grp: 2 (over x), ep: 16 (over z, y, core).
Axes of the slice: x: 2, y: 2, z: 4, core: 2. Of those that a mesh axis runs over, the one named last changes fastest.
Arguments:
- hidden: bfloat16 [224, 2048], P(('grp', 'ep')), parts along dimension 0, may hold values from -6 to 6
- state_in: float32 [224, 64, 4096], P(('grp', 'ep')), parts along dimension 0, may hold values from -4 to 4
- conv_state: bfloat16 [224, 3, 4608], P(('grp', 'ep')), parts along dimension 0, may hold values from -6 to 6
- expert_ids: int32 [224, 4], P(('grp', 'ep')), parts along dimension 0, may hold values from 0 to 15, as said below
- group_prob: float32 [224], P(('grp', 'ep')), parts along dimension 0, may hold values from 0.25 to 1
- expert_score: float32 [224, 4], P(('grp', 'ep')), parts along dimension 0, may hold values from 0.05 to 1
- first_gain: bfloat16 [2048], replicated, may hold values from 0.099609375 to 1.8984375
- z_weight: bfloat16 [2048, 4096], P(None, 'ep'), may hold values from -0.125 to 0.125
- x_weight: bfloat16 [2048, 4096], P(None, 'ep'), may hold values from -0.125 to 0.125
- b_weight: bfloat16 [2048, 256], replicated, may hold values from -0.125 to 0.125
- c_weight: bfloat16 [2048, 256], replicated, may hold values from -0.125 to 0.125
- dt_weight: bfloat16 [2048, 64], replicated, may hold values from -0.125 to 0.125
- conv_weight: bfloat16 [4, 4608], replicated, may hold values from -3 to 3
- conv_bias: bfloat16 [4608], replicated, may hold values from -3 to 3
- dt_bias: float32 [64], replicated, may hold values from -4 to 0
- decay_log: float32 [64], replicated, may hold values from 0 to 2
- skip_gain: float32 [64], replicated, may hold values from 0.1 to 1.9
- inner_gain: bfloat16 [4096], replicated, may hold values from 0.099609375 to 1.8984375
- out_weight: bfloat16 [4096, 2048], P(None, 'ep'), may hold values from -0.09375 to 0.09375
- second_gain: bfloat16 [2048], replicated, may hold values from 0.099609375 to 1.8984375
- expert_gate: bfloat16 [16, 2048, 512], P('ep'), may hold values from -0.125 to 0.125
- expert_up: bfloat16 [16, 2048, 512], P('ep'), may hold values from -0.125 to 0.125
- expert_down: bfloat16 [16, 512, 2048], P('ep'), may hold values from -0.25 to 0.25
Outputs:
- layer_out: bfloat16 [224, 2048], P(('grp', 'ep')), parts along dimension 0
- state_out: float32 [224, 64, 4096], P(('grp', 'ep')), parts along dimension 0
- conv_out: bfloat16 [224, 3, 4608], P(('grp', 'ep')), parts along dimension 0
There are 2 independent parts, one for each index of `grp`. A program takes and returns all parts, laid end to end along the dimension named above; an argument that names none is the same for every part. Nothing has to cross between parts.
Inputs may be any that keep to these rules, and one draw needn't show every extreme that they name: `expert_ids`: each row names 4 different experts of one expert group (numbers g * 8 to g * 8 + 7). Among the 7 rows of one device no expert is named more than 3 times, and in every draw one expert is named exactly 3 times by the rows of every device.
All inputs are finite; a program needn't handle non-finite values.
Results may differ from a plain program's by a relative error of at most 0.014.
Values may be sent and summed in bfloat16 or wider, within the bound.
No kernel may reach another device: no remote copies, remote signals or barrier semaphores. Data moves between devices by JAX's collectives and lax.ppermute only.
A program may use at most 128 MiB of HBM per device.

v0:
```python
import jax
import jax.numpy as jnp
from jax import lax
from jax.sharding import PartitionSpec as P

HEADS = 64
HEAD_DIM = 64
SSM_GROUPS = 4
STATE = 64
TOP = 4
EPS = 1e-06


def rms_scale(values, gain_vec):
    return (
        values
        * lax.rsqrt(jnp.mean(values * values, axis=-1, keepdims=True) + EPS)
        * gain_vec.astype(jnp.float32)
    )


def state_step(active, dt_raw, state_in, dt_bias, decay_log, skip_gain):
    row_count = active.shape[0]
    inner_width = HEADS * HEAD_DIM
    state_span = SSM_GROUPS * STATE
    per_group = HEADS // SSM_GROUPS
    x_heads = active[:, :inner_width].reshape(row_count, HEADS, HEAD_DIM)
    b_input = active[:, inner_width : inner_width + state_span].reshape(
        row_count, SSM_GROUPS, STATE
    )
    c_input = active[:, inner_width + state_span :].reshape(row_count, SSM_GROUPS, STATE)
    b_heads = jnp.repeat(b_input, per_group, axis=1)
    c_heads = jnp.repeat(c_input, per_group, axis=1)
    step_size = jax.nn.softplus(dt_raw.astype(jnp.float32) + dt_bias[None, :])
    decay_rate = jnp.exp(-step_size * jnp.exp(decay_log)[None, :])
    carried = state_in.reshape(row_count, HEADS, HEAD_DIM, STATE)
    carried = (
        decay_rate[:, :, None, None] * carried
        + (step_size[:, :, None] * x_heads)[:, :, :, None] * b_heads[:, :, None, :]
    )
    readout = jnp.einsum("bhpn,bhn->bhp", carried, c_heads, precision=lax.Precision.HIGHEST)
    readout = readout + skip_gain[None, :, None] * x_heads
    return (
        readout.reshape(row_count, inner_width),
        carried.reshape(row_count, HEADS, HEAD_DIM * STATE),
    )


def body(
    hidden,
    state_in,
    conv_state,
    expert_ids,
    group_prob,
    expert_score,
    first_gain,
    z_weight,
    x_weight,
    b_weight,
    c_weight,
    dt_weight,
    conv_weight,
    conv_bias,
    dt_bias,
    decay_log,
    skip_gain,
    inner_gain,
    out_weight,
    second_gain,
    expert_gate,
    expert_up,
    expert_down,
):
    row_count = hidden.shape[0]
    model_width = hidden.shape[1]
    normed = rms_scale(hidden.astype(jnp.float32), first_gain).astype(jnp.bfloat16)
    row_part = lax.all_gather(normed, "ep", axis=0, tiled=True)
    both_parts = jnp.concatenate(
        [
            jnp.dot(row_part, z_weight, preferred_element_type=jnp.float32),
            jnp.dot(row_part, x_weight, preferred_element_type=jnp.float32),
        ],
        axis=1,
    )
    projected_both = both_parts.astype(jnp.bfloat16)
    col_count = z_weight.shape[1]
    gate_z, x_part = (
        lax.all_to_all(
            projected_both[:, :col_count], "ep", split_axis=0, concat_axis=1, tiled=True
        ),
        lax.all_to_all(
            projected_both[:, col_count:], "ep", split_axis=0, concat_axis=1, tiled=True
        ),
    )
    b_part = jnp.dot(normed, b_weight, preferred_element_type=jnp.float32).astype(jnp.bfloat16)
    c_part = jnp.dot(normed, c_weight, preferred_element_type=jnp.float32).astype(jnp.bfloat16)
    dt_raw = jnp.dot(normed, dt_weight, preferred_element_type=jnp.float32).astype(jnp.bfloat16)
    fresh_input = jnp.concatenate([x_part, b_part, c_part], axis=1)
    window = jnp.concatenate([conv_state, fresh_input[:, None, :]], axis=1)
    summed = jnp.sum(window.astype(jnp.float32) * conv_weight.astype(jnp.float32)[None], axis=1)
    active = jax.nn.silu(summed + conv_bias.astype(jnp.float32)[None, :])
    readout, state_out = state_step(active, dt_raw, state_in, dt_bias, decay_log, skip_gain)
    gated = readout * jax.nn.silu(gate_z.astype(jnp.float32))
    y_mix = rms_scale(gated, inner_gain).astype(jnp.bfloat16)
    slice_out = jnp.dot(
        lax.all_gather(y_mix, "ep", axis=0, tiled=True),
        out_weight,
        preferred_element_type=jnp.float32,
    ).astype(jnp.bfloat16)
    projected = lax.all_to_all(slice_out, "ep", split_axis=0, concat_axis=1, tiled=True)
    projected = lax.optimization_barrier(projected)
    mixed_rows = (hidden.astype(jnp.float32) + projected.astype(jnp.float32)).astype(jnp.bfloat16)
    normed2 = rms_scale(mixed_rows.astype(jnp.float32), second_gain).astype(jnp.bfloat16)
    expert_count = lax.axis_size("ep")
    capacity = max(2, (3 * row_count * TOP + 2 * expert_count - 1) // (2 * expert_count))
    slot_total = expert_count * capacity
    flat_ids = expert_ids.reshape(-1)
    one_hot = (flat_ids[:, None] == jnp.arange(expert_count, dtype=jnp.int32)[None, :]).astype(
        jnp.int32
    )
    earlier = jnp.cumsum(one_hot, axis=0) - one_hot
    slot_rank = jnp.sum(earlier * one_hot, axis=1)
    slot_place = (flat_ids * capacity + slot_rank).reshape(row_count, TOP)
    slot_index = jnp.arange(slot_total, dtype=jnp.int32)
    dispatch = jnp.sum(
        (slot_index[:, None, None] == slot_place[None, :, :]).astype(jnp.int32), axis=2
    )
    outgoing = jnp.dot(dispatch.astype(jnp.bfloat16), normed2, preferred_element_type=jnp.float32)
    outgoing = outgoing.astype(jnp.bfloat16).reshape(expert_count, capacity, model_width)
    arrived = lax.all_to_all(outgoing, "ep", split_axis=0, concat_axis=0, tiled=True)
    sources, slots_here, width = arrived.shape
    flattened = arrived.reshape(sources * slots_here, width)
    gate_part = jnp.dot(flattened, expert_gate[0], preferred_element_type=jnp.float32)
    up_part = jnp.dot(flattened, expert_up[0], preferred_element_type=jnp.float32)
    hidden_act = (jax.nn.silu(gate_part) * up_part).astype(jnp.bfloat16)
    expert_out = jnp.dot(hidden_act, expert_down[0], preferred_element_type=jnp.float32).astype(
        jnp.bfloat16
    )
    returned = lax.all_to_all(
        expert_out.reshape(sources, slots_here, width),
        "ep",
        split_axis=0,
        concat_axis=0,
        tiled=True,
    )
    returned = returned.reshape(slot_total, model_width)
    route_share = group_prob[:, None] * expert_score / jnp.sum(expert_score, axis=1, keepdims=True)
    moe_sum = jnp.zeros((row_count, model_width), jnp.float32)
    for pick in range(TOP):
        select_rows = (slot_place[:, pick][:, None] == slot_index[None, :]).astype(jnp.bfloat16)
        picked = jnp.dot(select_rows, returned, preferred_element_type=jnp.float32)
        moe_sum = moe_sum + route_share[:, pick : pick + 1] * picked
    layer_out = (mixed_rows.astype(jnp.float32) + moe_sum).astype(jnp.bfloat16)
    return (layer_out, state_out, window[:, 1:, :])


def solution(mesh):
    in_specs = (
        P(("grp", "ep"), None),
        P(("grp", "ep"), None, None),
        P(("grp", "ep"), None, None),
        P(("grp", "ep"), None),
        P(("grp", "ep")),
        P(("grp", "ep"), None),
        P(),
        P(None, "ep"),
        P(None, "ep"),
        P(),
        P(),
        P(),
        P(),
        P(),
        P(),
        P(),
        P(),
        P(),
        P(None, "ep"),
        P(),
        P("ep", None, None),
        P("ep", None, None),
        P("ep", None, None),
    )
    out_specs = (P(("grp", "ep"), None), P(("grp", "ep"), None, None), P(("grp", "ep"), None, None))
    return jax.shard_map(body, mesh=mesh, in_specs=in_specs, out_specs=out_specs, check_vma=False)
```

profile of v0, /device:TPU:0, one launch (start us, length us, event | category | flops | bytes accessed | tf_op | source)
XLA Modules:
  0.0 186.1 jit_solution(1612493214570379041)
XLA Ops:
  0.6 0.8 convert_element_type.99
  1.5 0.9 fusion.30
  2.4 0.8 fusion.52
  3.2 24.6 %all-gather = bf16[16,7,2048]{2,1,0:T(8,128)(2,1)S(1)} all-gather(bf16[1,7,2048]{2,1,0:T(8,128)(2,1)S(1)} %fusion.52), channel_id=1, replica_groups=mesh['grp'=2,'ep'=16] {'ep'}, dimensions={0}, use_global_device_ids=true | all-gather | bytes 487424 | tf_op jit(solution)/shard_map/all_gather | solution.py:77
  28.0 1.5 convolution_convert_fusion.3
  30.2 3.5 %all-to-all-start = ((bf16[16,7,256]{2,1,0:T(8,128)(2,1)}), bf16[16,7,256]{2,1,0:T(8,128)(2,1)S(1)}, u32[]{:S(2)}, u32[]{:S(2)}) async-start(bf16[16,7,256]{2,1,0:T(8,128)(2,1)} %all_to_all.44), calls=%async_computation | async-start | bytes 131072 | tf_op jit(solution)/shard_map/all_to_all | solution.py:91
  33.7 1.5 convolution_convert_fusion.5
  35.2 1.5 convolution_convert_fusion.6
  36.7 0.8 convert_element_type.106
  37.5 0.7 convert_element_type.107
  39.0 12.7 %reshape.106 = f32[7,64,64,64]{3,2,1,0:T(8,128)} reshape(f32[7,64,4096]{2,1,0:T(8,128)} %param.24) | data formatting | bytes 14680064 | tf_op jit(solution)/shard_map/reshape | solution.py:36
  51.7 1.5 convolution_convert_fusion.2
  53.3 0.7 all_to_all.48
  55.2 6.0 %all-to-all-start.1 = ((bf16[16,7,256]{2,1,0:T(8,128)(2,1)}), bf16[16,7,256]{2,1,0:T(8,128)(2,1)S(1)}, u32[]{:S(2)}, u32[]{:S(2)}) async-start(bf16[16,7,256]{2,1,0:T(8,128)(2,1)} %all_to_all.48), calls=%async_computation.1 | async-start | bytes 131072 | tf_op jit(solution)/shard_map/all_to_all | solution.py:88
  61.7 6.4 %all-to-all-done.1 = bf16[16,7,256]{2,1,0:T(8,128)(2,1)S(1)} async-done(((bf16[16,7,256]{2,1,0:T(8,128)(2,1)}), bf16[16,7,256]{2,1,0:T(8,128)(2,1)S(1)}, u32[]{:S(2)}, u32[]{:S(2)}) %all-to-all-start.1) | async-done | bytes 57376 | tf_op jit(solution)/shard_map/all_to_all | solution.py:88
  68.5 26.7 %fusion = f32[7,64,1,64]{3,2,1,0:T(1,128)S(1)} fusion(f32[7,64,64,1]{2,3,1,0:T(1,128)S(1)} %bitcast.68, f32[7,64,64,64]{3,2,1,0:T(8,128)} %reshape.106, f32[7,64]{1,0:T(8,128)S(1)} %get-tuple-element.17, f32[7,64,64]{2,1,0:T(8,128)S(1)} %bitcast.65, f32[7,64,64]{2,1,0:T(8,128)S(1)} %broadcast_multiply_fusion.2), kind=kOutput, calls=%fused_computation | convolution fusion | flops 27525120 | bytes 7800576 | tf_op jit(solution)/shard_map/bhpn,bhn->bhp/dot_general | solution.py:41
  95.6 20.7 %all-gather.1 = bf16[16,7,4096]{2,1,0:T(8,128)(2,1)S(1)} all-gather(bf16[1,7,4096]{2,1,0:T(8,128)(2,1)S(1)} %fusion.37), channel_id=1, replica_groups=mesh['grp'=2,'ep'=16] {'ep'}, dimensions={0}, use_global_device_ids=true | all-gather | bytes 974848 | tf_op jit(solution)/shard_map/all_gather | solution.py:106
  116.3 1.2 reshape.121
  117.6 1.9 %convolution_convert_fusion.4 = bf16[112,128]{1,0:T(8,128)(2,1)S(1)} fusion(bf16[112,4096]{1,0:T(8,128)(2,1)} %reshape.121, bf16[4096,128]{1,0:T(8,128)(2,1)} %param.41), kind=kOutput, calls=%fused_computation.26 | convolution fusion | flops 117454848 | bytes 1994752 | tf_op jit(solution)/shard_map/dot_general | solution.py:105
  120.1 3.5 %all-to-all-start.2 = ((bf16[16,7,128]{2,1,0:T(8,128)(2,1)}), bf16[16,7,128]{2,1,0:T(8,128)(2,1)S(1)}, u32[]{:S(2)}, u32[]{:S(2)}) async-start(bf16[16,7,128]{2,1,0:T(8,128)(2,1)} %all_to_all.50), calls=%async_computation.2 | async-start | bytes 65536 | tf_op jit(solution)/shard_map/all_to_all | solution.py:110
  123.6 8.7 %broadcast_multiply_fusion = f32[7,64,64,64]{3,2,1,0:T(8,128)} fusion(f32[7,64,64]{2,1,0:T(8,128)} %bitcast.66, f32[7,64,64]{2,1,0:T(8,128)S(1)} %broadcast_multiply_fusion.2), kind=kLoop, calls=%fused_computation.4 | loop fusion | flops 1835008 | bytes 7569408 | tf_op jit(solution)/shard_map/mul | solution.py:39
  132.3 12.9 %mul.261 = f32[7,64,4096]{2,1,0:T(8,128)} reshape(f32[7,64,64,64]{3,2,1,0:T(8,128)} %broadcast_multiply_fusion) | data formatting | bytes 14680064 | tf_op jit(solution)/shard_map/mul | solution.py:39
  145.6 0.8 reshape.112
  146.4 6.0 %all-to-all-start.3 = ((bf16[16,3,2048]{2,1,0:T(4,128)(2,1)}), bf16[16,3,2048]{2,1,0:T(4,128)(2,1)S(1)}, u32[]{:S(2)}, u32[]{:S(2)}) async-start(bf16[16,3,2048]{2,1,0:T(4,128)(2,1)} %reshape.112), calls=%async_computation.3 | async-start | bytes 524288 | tf_op jit(solution)/shard_map/all_to_all | solution.py:130
  152.4 10.6 %multiply_add_fusion = f32[7,64,4096]{2,1,0:T(8,128)} fusion(f32[7,64,4096]{2,1,0:T(8,128)} %mul.261, f32[7,64,4096]{2,1,0:T(8,128)} %param.24, f32[7,64]{1,0:T(8,128)S(1)} %get-tuple-element.17), kind=kLoop, calls=%fused_computation.3 | loop fusion | flops 3670016 | bytes 22021888 | tf_op jit(solution)/shard_map/add | solution.py:38
  163.1 2.0 %fusion.12 = f32[48,512]{1,0:T(8,128)S(1)} fusion(bf16[48,2048]{1,0:T(8,128)(2,1)S(1)} %reshape.113, bf16[1,2048,512]{2,1,0:T(8,128)(2,1)} %param.43), kind=kOutput, calls=%fused_computation.20 | convolution fusion | flops 100663296 | bytes 2392064 | tf_op jit(solution)/shard_map/dot_general | solution.py:133
  165.2 2.5 %convolution_convert_fusion = bf16[48,2048]{1,0:T(8,128)(2,1)S(1)} fusion(bf16[1,512,2048]{2,1,0:T(8,128)(2,1)S(1)} %copy-done, bf16[48,2048]{1,0:T(8,128)(2,1)S(1)} %reshape.113, bf16[1,2048,512]{2,1,0:T(8,128)(2,1)} %param.44, f32[48,512]{1,0:T(8,128)S(1)} %fusion.12), kind=kOutput, calls=%fused_computation.6 | convolution fusion | flops 201572352 | bytes 4685824 | tf_op jit(solution)/shard_map/dot_general | solution.py:136
  167.7 0.8 reshape.114
  168.5 6.0 %all-to-all-start.4 = ((bf16[16,3,2048]{2,1,0:T(4,128)(2,1)}), bf16[16,3,2048]{2,1,0:T(4,128)(2,1)S(1)}, u32[]{:S(2)}, u32[]{:S(2)}) async-start(bf16[16,3,2048]{2,1,0:T(4,128)(2,1)} %reshape.114), calls=%async_computation.4 | async-start | bytes 524288 | tf_op jit(solution)/shard_map/all_to_all | solution.py:139
  174.5 0.7 fusion.24
  175.3 9.3 %all-to-all-done.4 = bf16[16,3,2048]{2,1,0:T(4,128)(2,1)S(1)} async-done(((bf16[16,3,2048]{2,1,0:T(4,128)(2,1)}), bf16[16,3,2048]{2,1,0:T(4,128)(2,1)S(1)}, u32[]{:S(2)}, u32[]{:S(2)}) %all-to-all-start.4) | async-done | bytes 196640 | tf_op jit(solution)/shard_map/all_to_all | solution.py:139
  185.3 0.8 fusion.8
  (75 shorter events, 5.9 us)
Async XLA Ops:
  0.6 164.5 %copy-start = (bf16[1,512,2048]{2,1,0:T(8,128)(2,1)S(1)}, bf16[1,512,2048]{2,1,0:T(8,128)(2,1)}, u32[]{:S(2)}) copy-start(bf16[1,512,2048]{2,1,0:T(8,128)(2,1)} %param.45) | copy-start | bytes 6291460
  30.2 25.0 %all-to-all-start = ((bf16[16,7,256]{2,1,0:T(8,128)(2,1)}), bf16[16,7,256]{2,1,0:T(8,128)(2,1)S(1)}, u32[]{:S(2)}, u32[]{:S(2)}) async-start(bf16[16,7,256]{2,1,0:T(8,128)(2,1)} %all_to_all.44), calls=%async_computation | async-start | bytes 131072 | tf_op jit(solution)/shard_map/all_to_all | solution.py:91
  38.9 15.0 %copy-start.5 = (bf16[4096]{0:T(1024)(128)(2,1)S(1)}, bf16[4096]{0:T(1024)(128)(2,1)}, u32[]{:S(2)}) copy-start(bf16[4096]{0:T(1024)(128)(2,1)} %param.40) | copy-start | bytes 24580
  38.9 15.0 %copy-start.8 = (s32[7,4]{0,1:T(4,128)S(1)}, s32[7,4]{0,1:T(4,128)}, u32[]{:S(2)}) copy-start(s32[7,4]{0,1:T(4,128)} %param.26) | copy-start | bytes 340
  38.9 15.7 %copy-start.7 = (bf16[2048]{0:T(1024)(128)(2,1)S(1)}, bf16[2048]{0:T(1024)(128)(2,1)}, u32[]{:S(2)}) copy-start(bf16[2048]{0:T(1024)(128)(2,1)} %param.42) | copy-start | bytes 12292
  38.9 15.7 %copy-start.6 = (f32[7,4]{0,1:T(4,128)S(1)}, f32[7,4]{0,1:T(4,128)}, u32[]{:S(2)}) copy-start(f32[7,4]{0,1:T(4,128)} %param.28) | copy-start | bytes 340
  38.9 15.7 %copy-start.10 = (f32[7]{0:T(128)S(1)}, f32[7]{0:T(128)}, u32[]{:S(2)}) copy-start(f32[7]{0:T(128)} %param.27) | copy-start | bytes 88
  38.9 15.8 %copy-start.2 = (bf16[7,2048]{1,0:T(8,128)(2,1)S(1)}, bf16[7,2048]{1,0:T(8,128)(2,1)}, u32[]{:S(2)}) copy-start(bf16[7,2048]{1,0:T(8,128)(2,1)} %param.23) | copy-start | bytes 86020
  38.9 15.8 %copy-start.11 = (bf16[2048,64]{0,1:T(8,128)(2,1)S(1)}, bf16[2048,64]{0,1:T(8,128)(2,1)}, u32[]{:S(2)}) copy-start(bf16[2048,64]{0,1:T(8,128)(2,1)} %param.34) | copy-start | bytes 786436
  39.0 15.8 %copy-start.12 = (f32[64]{0:T(128)S(1)}, f32[64]{0:T(128)}, u32[]{:S(2)}) copy-start(f32[64]{0:T(128)} %param.37) | copy-start | bytes 772
  39.0 22.3 %copy-start.3 = (bf16[7,3,4608]{2,0,1:T(8,128)(2,1)S(1)}, bf16[7,3,4608]{2,0,1:T(8,128)(2,1)}, u32[]{:S(2)}) copy-start(bf16[7,3,4608]{2,0,1:T(8,128)(2,1)} %param.25) | copy-start | bytes 580612
  55.2 12.9 %all-to-all-start.1 = ((bf16[16,7,256]{2,1,0:T(8,128)(2,1)}), bf16[16,7,256]{2,1,0:T(8,128)(2,1)S(1)}, u32[]{:S(2)}, u32[]{:S(2)}) async-start(bf16[16,7,256]{2,1,0:T(8,128)(2,1)} %all_to_all.48), calls=%async_computation.1 | async-start | bytes 131072 | tf_op jit(solution)/shard_map/all_to_all | solution.py:88
  68.4 26.7 %copy-start.1 = (f32[7,4,16,64]{3,2,1,0:T(8,128)}, f32[7,4,16,64]{3,2,1,0:T(8,128)S(1)}, u32[]{:S(2)}) copy-start(f32[7,4,16,64]{3,2,1,0:T(8,128)S(1)} %broadcast_in_dim.7) | copy-start | bytes 344068
  68.5 26.7 %copy-start.9 = (f32[64]{0:T(128)S(1)}, f32[64]{0:T(128)}, u32[]{:S(2)}) copy-start(f32[64]{0:T(128)} %param.39) | copy-start | bytes 772
  120.1 25.1 %all-to-all-start.2 = ((bf16[16,7,128]{2,1,0:T(8,128)(2,1)}), bf16[16,7,128]{2,1,0:T(8,128)(2,1)S(1)}, u32[]{:S(2)}, u32[]{:S(2)}) async-start(bf16[16,7,128]{2,1,0:T(8,128)(2,1)} %all_to_all.50), calls=%async_computation.2 | async-start | bytes 65536 | tf_op jit(solution)/shard_map/all_to_all | solution.py:110
  146.4 16.6 %all-to-all-start.3 = ((bf16[16,3,2048]{2,1,0:T(4,128)(2,1)}), bf16[16,3,2048]{2,1,0:T(4,128)(2,1)S(1)}, u32[]{:S(2)}, u32[]{:S(2)}) async-start(bf16[16,3,2048]{2,1,0:T(4,128)(2,1)} %reshape.112), calls=%async_computation.3 | async-start | bytes 524288 | tf_op jit(solution)/shard_map/all_to_all | solution.py:130
  162.9 11.6 %copy-start.4 = (bf16[7,3,4608]{2,0,1:T(8,128)(2,1)S(1)}, bf16[7,3,4608]{2,0,1:T(8,128)(2,1)}, u32[]{:S(2)}) copy-start(bf16[7,3,4608]{2,0,1:T(8,128)(2,1)} %param.25) | copy-start | bytes 580612
  168.5 16.0 %all-to-all-start.4 = ((bf16[16,3,2048]{2,1,0:T(4,128)(2,1)}), bf16[16,3,2048]{2,1,0:T(4,128)(2,1)S(1)}, u32[]{:S(2)}, u32[]{:S(2)}) async-start(bf16[16,3,2048]{2,1,0:T(4,128)(2,1)} %reshape.114), calls=%async_computation.4 | async-start | bytes 524288 | tf_op jit(solution)/shard_map/all_to_all | solution.py:139
where the time goes:
time: 188 us; the launch traced here: 186 us
  blocking collectives  45.3 us (24%)
  matrix products  41.2 us (22%)
  local copies, waits for them, and re-layouts  32.7 us (17%)
  other arithmetic  25.3 us (13%)
  starting transfers between devices  25 us (13%)
  waiting for transfers between devices  15.7 us (8%)
    dot_general x1, matrix products, state_step(): jnp.einsum('bhpn,bhn->bhp', carried, c_heads, precision=lax.Precision.HIG...  26.7 us
    all_gather x1, blocking collectives, body(): row_part = lax.all_gather(normed, 'ep', axis=0, tiled=True)  24.6 us
    all_gather x1, blocking collectives, body(): lax.all_gather(y_mix, 'ep', axis=0, tiled=True)  20.7 us
    mul x1, local copies, waits for them, and re-layouts, state_step(): (step_size[:, :, None] * x_heads)[:, :, :, None] * b_heads[:, :, None, :]  12.9 us
    reshape x1, local copies, waits for them, and re-layouts, state_step(): carried = state_in.reshape(row_count, HEADS, HEAD_DIM, STATE)  12.7 us
    add x1, other arithmetic, state_step(): decay_rate[:, :, None, None] * carried  10.6 us
    all_to_all x1, waiting for transfers between devices, body(): lax.all_to_all(expert_out.reshape(sources, slots_here, width), 'ep', spli...  9.27 us
    mul x1, other arithmetic, state_step(): (step_size[:, :, None] * x_heads)[:, :, :, None] * b_heads[:, :, None, :]  8.67 us
  transfers between devices with their start and end apart: 5, of which 2 were waited for; matrix products, arithmetic and copies ran while one was open for 29% of the time, Pallas kernels for 0%

commit v1 on v0

--- a/solution.py
+++ b/solution.py
@@ -85,8 +85,14 @@
     projected_both = both_parts.astype(jnp.bfloat16)
     col_count = z_weight.shape[1]
     gate_z, x_part = (
-        lax.all_to_all(
-            projected_both[:, :col_count], "ep", split_axis=0, concat_axis=1, tiled=True
+        jnp.concatenate(
+            lax.all_to_all(
+                jnp.stack(jnp.split(projected_both[:, :col_count], lax.axis_size("ep"), axis=0)),
+                "ep",
+                0,
+                0,
+            ),
+            axis=1,
         ),
         lax.all_to_all(
             projected_both[:, col_count:], "ep", split_axis=0, concat_axis=1, tiled=True

time: 188 us -> 195 us (1.037)
  local copies, waits for them, and re-layouts: 32.7 us -> 41 us
    unnamed x29 -> x50, local copies, waits for them, and re-layouts: 1.58 us -> 10.5 us
  transfers between devices with their start and end apart: 5 -> 5, of which waited for: 2 -> 2; matrix products, arithmetic and copies ran while one was open for 29% -> 32% of each run, Pallas kernels for 0% -> 0%
where the time goes in v1:
time: 195 us; the launch traced here: 193 us
  blocking collectives  45.3 us (23%)
  matrix products  41.2 us (21%)
  local copies, waits for them, and re-layouts  41 us (21%)
  starting transfers between devices  25 us (13%)
  other arithmetic  23.8 us (12%)
  waiting for transfers between devices  15.9 us (8%)
    dot_general x1, matrix products, state_step(): jnp.einsum('bhpn,bhn->bhp', carried, c_heads, precision=lax.Precision.HIG...  26.7 us
    all_gather x1, blocking collectives, body(): row_part = lax.all_gather(normed, 'ep', axis=0, tiled=True)  24.6 us
    all_gather x1, blocking collectives, body(): lax.all_gather(y_mix, 'ep', axis=0, tiled=True)  20.7 us
    mul x1, local copies, waits for them, and re-layouts, state_step(): (step_size[:, :, None] * x_heads)[:, :, :, None] * b_heads[:, :, None, :]  12.9 us
    reshape x1, local copies, waits for them, and re-layouts, state_step(): carried = state_in.reshape(row_count, HEADS, HEAD_DIM, STATE)  12.7 us
    add x1, other arithmetic, state_step(): decay_rate[:, :, None, None] * carried  10.6 us
    unnamed x50, local copies, waits for them, and re-layouts  10.5 us
    all_to_all x1, waiting for transfers between devices, body(): lax.all_to_all(expert_out.reshape(sources, slots_here, width), 'ep', spli...  9.27 us
  transfers between devices with their start and end apart: 5, of which 2 were waited for; matrix products, arithmetic and copies ran while one was open for 32% of the time, Pallas kernels for 0%

profile of v1, /device:TPU:0, one launch (start us, length us, event | category | flops | bytes accessed | tf_op | source)
XLA Modules:
  0.0 193.2 jit_solution(4108040612240752034)
XLA Ops:
  0.7 0.8 convert_element_type.99
  1.5 0.9 fusion.30
  2.4 0.8 fusion.52
  3.2 24.6 %all-gather = bf16[16,7,2048]{2,1,0:T(8,128)(2,1)S(1)} all-gather(bf16[1,7,2048]{2,1,0:T(8,128)(2,1)S(1)} %fusion.52), channel_id=1, replica_groups=mesh['grp'=2,'ep'=16] {'ep'}, dimensions={0}, use_global_device_ids=true | all-gather | bytes 487424 | tf_op jit(solution)/shard_map/all_gather | solution.py:77
  28.0 1.5 convolution_convert_fusion.3
  29.5 0.7 all_to_all.37
  30.2 3.5 %all-to-all-start = ((bf16[16,7,256]{2,1,0:T(8,128)(2,1)}), bf16[16,7,256]{2,1,0:T(8,128)(2,1)S(1)}, u32[]{:S(2)}, u32[]{:S(2)}) async-start(bf16[16,7,256]{2,1,0:T(8,128)(2,1)} %all_to_all.37), calls=%async_computation | async-start | bytes 131072 | tf_op jit(solution)/shard_map/all_to_all | solution.py:97
  33.7 1.5 convolution_convert_fusion.2
  36.4 0.6 constant_dynamic-update-slice_fusion.13
  44.8 1.5 convolution_convert_fusion.5
  46.3 1.5 convolution_convert_fusion.6
  48.0 12.7 %reshape.105 = f32[7,64,64,64]{3,2,1,0:T(8,128)} reshape(f32[7,64,4096]{2,1,0:T(8,128)} %param.24) | data formatting | bytes 14680064 | tf_op jit(solution)/shard_map/reshape | solution.py:36
  62.1 6.0 %all-to-all-start.1 = ((bf16[16,7,256]{2,1,0:T(8,128)(2,1)}), bf16[16,7,256]{2,1,0:T(8,128)(2,1)S(1)}, u32[]{:S(2)}, u32[]{:S(2)}) async-start(bf16[16,7,256]{2,1,0:T(8,128)(2,1)} %constant_dynamic-update-slice_fusion), calls=%async_computation.1 | async-start | bytes 131072 | tf_op jit(solution)/shard_map/all_to_all | solution.py:89
  68.3 6.7 %all-to-all-done.1 = bf16[16,7,256]{2,1,0:T(8,128)(2,1)S(1)} async-done(((bf16[16,7,256]{2,1,0:T(8,128)(2,1)}), bf16[16,7,256]{2,1,0:T(8,128)(2,1)S(1)}, u32[]{:S(2)}, u32[]{:S(2)}) %all-to-all-start.1) | async-done | bytes 57376 | tf_op jit(solution)/shard_map/all_to_all | solution.py:89
  75.6 26.7 %fusion = f32[7,64,1,64]{3,2,1,0:T(1,128)S(1)} fusion(f32[7,64,64,1]{2,3,1,0:T(1,128)S(1)} %bitcast.132, f32[7,64,64,64]{3,2,1,0:T(8,128)} %reshape.105, f32[7,64]{1,0:T(8,128)S(1)} %get-tuple-element.17, f32[7,64,64]{2,1,0:T(8,128)S(1)} %bitcast.129, f32[7,64,64]{2,1,0:T(8,128)S(1)} %broadcast_multiply_fusion.2), kind=kOutput, calls=%fused_computation | convolution fusion | flops 27525120 | bytes 7800576 | tf_op jit(solution)/shard_map/bhpn,bhn->bhp/dot_general | solution.py:41
  102.7 20.7 %all-gather.1 = bf16[16,7,4096]{2,1,0:T(8,128)(2,1)S(1)} all-gather(bf16[1,7,4096]{2,1,0:T(8,128)(2,1)S(1)} %fusion.37), channel_id=1, replica_groups=mesh['grp'=2,'ep'=16] {'ep'}, dimensions={0}, use_global_device_ids=true | all-gather | bytes 974848 | tf_op jit(solution)/shard_map/all_gather | solution.py:112
  123.4 1.2 reshape.120
  124.6 1.9 convolution_convert_fusion.4
  126.5 0.6 all_to_all.42
  127.2 3.5 %all-to-all-start.2 = ((bf16[16,7,128]{2,1,0:T(8,128)(2,1)}), bf16[16,7,128]{2,1,0:T(8,128)(2,1)S(1)}, u32[]{:S(2)}, u32[]{:S(2)}) async-start(bf16[16,7,128]{2,1,0:T(8,128)(2,1)} %all_to_all.42), calls=%async_computation.2 | async-start | bytes 65536 | tf_op jit(solution)/shard_map/all_to_all | solution.py:116
  130.7 8.7 %broadcast_multiply_fusion = f32[7,64,64,64]{3,2,1,0:T(8,128)} fusion(f32[7,64,64]{2,1,0:T(8,128)} %bitcast.130, f32[7,64,64]{2,1,0:T(8,128)S(1)} %broadcast_multiply_fusion.2), kind=kLoop, calls=%fused_computation.4 | loop fusion | flops 1835008 | bytes 7569408 | tf_op jit(solution)/shard_map/mul | solution.py:39
  139.4 12.9 %mul.261 = f32[7,64,4096]{2,1,0:T(8,128)} reshape(f32[7,64,64,64]{3,2,1,0:T(8,128)} %broadcast_multiply_fusion) | data formatting | bytes 14680064 | tf_op jit(solution)/shard_map/mul | solution.py:39
  152.7 0.8 reshape.111
  153.5 6.0 %all-to-all-start.3 = ((bf16[16,3,2048]{2,1,0:T(4,128)(2,1)}), bf16[16,3,2048]{2,1,0:T(4,128)(2,1)S(1)}, u32[]{:S(2)}, u32[]{:S(2)}) async-start(bf16[16,3,2048]{2,1,0:T(4,128)(2,1)} %reshape.111), calls=%async_computation.3 | async-start | bytes 524288 | tf_op jit(solution)/shard_map/all_to_all | solution.py:136
  159.5 10.6 %multiply_add_fusion = f32[7,64,4096]{2,1,0:T(8,128)} fusion(f32[7,64,4096]{2,1,0:T(8,128)} %mul.261, f32[7,64,4096]{2,1,0:T(8,128)} %param.24, f32[7,64]{1,0:T(8,128)S(1)} %get-tuple-element.17), kind=kLoop, calls=%fused_computation.3 | loop fusion | flops 3670016 | bytes 22021888 | tf_op jit(solution)/shard_map/add | solution.py:38
  170.2 2.0 %fusion.12 = f32[48,512]{1,0:T(8,128)S(1)} fusion(bf16[48,2048]{1,0:T(8,128)(2,1)S(1)} %reshape.112, bf16[1,2048,512]{2,1,0:T(8,128)(2,1)} %param.43), kind=kOutput, calls=%fused_computation.20 | convolution fusion | flops 100663296 | bytes 2392064 | tf_op jit(solution)/shard_map/dot_general | solution.py:139
  172.3 2.5 %convolution_convert_fusion = bf16[48,2048]{1,0:T(8,128)(2,1)S(1)} fusion(bf16[1,512,2048]{2,1,0:T(8,128)(2,1)S(1)} %copy-done, bf16[48,2048]{1,0:T(8,128)(2,1)S(1)} %reshape.112, bf16[1,2048,512]{2,1,0:T(8,128)(2,1)} %param.44, f32[48,512]{1,0:T(8,128)S(1)} %fusion.12), kind=kOutput, calls=%fused_computation.6 | convolution fusion | flops 201572352 | bytes 4685824 | tf_op jit(solution)/shard_map/dot_general | solution.py:142
  174.8 0.8 reshape.113
  175.6 6.0 %all-to-all-start.4 = ((bf16[16,3,2048]{2,1,0:T(4,128)(2,1)}), bf16[16,3,2048]{2,1,0:T(4,128)(2,1)S(1)}, u32[]{:S(2)}, u32[]{:S(2)}) async-start(bf16[16,3,2048]{2,1,0:T(4,128)(2,1)} %reshape.113), calls=%async_computation.4 | async-start | bytes 524288 | tf_op jit(solution)/shard_map/all_to_all | solution.py:145
  181.6 0.7 fusion.24
  182.4 9.3 %all-to-all-done.4 = bf16[16,3,2048]{2,1,0:T(4,128)(2,1)S(1)} async-done(((bf16[16,3,2048]{2,1,0:T(4,128)(2,1)}), bf16[16,3,2048]{2,1,0:T(4,128)(2,1)S(1)}, u32[]{:S(2)}, u32[]{:S(2)}) %all-to-all-start.4) | async-done | bytes 196640 | tf_op jit(solution)/shard_map/all_to_all | solution.py:145
  192.4 0.8 fusion.8
  (96 shorter events, 13.0 us)
Async XLA Ops:
  0.6 171.6 %copy-start = (bf16[1,512,2048]{2,1,0:T(8,128)(2,1)S(1)}, bf16[1,512,2048]{2,1,0:T(8,128)(2,1)}, u32[]{:S(2)}) copy-start(bf16[1,512,2048]{2,1,0:T(8,128)(2,1)} %param.45) | copy-start | bytes 6291460
  0.6 47.2 %copy-start.5 = (bf16[4,4608]{1,0:T(4,128)(2,1)S(1)}, bf16[4,4608]{1,0:T(4,128)(2,1)}, u32[]{:S(2)}) copy-start(bf16[4,4608]{1,0:T(4,128)(2,1)} %param.35) | copy-start | bytes 110596
  0.7 47.2 %copy-start.6 = (bf16[4608]{0:T(1024)(128)(2,1)S(1)}, bf16[4608]{0:T(1024)(128)(2,1)}, u32[]{:S(2)}) copy-start(bf16[4608]{0:T(1024)(128)(2,1)} %param.36) | copy-start | bytes 27652
  0.7 47.2 %copy-start.14 = (f32[64]{0:T(128)S(1)}, f32[64]{0:T(128)}, u32[]{:S(2)}) copy-start(f32[64]{0:T(128)} %param.38) | copy-start | bytes 772
  30.2 31.8 %all-to-all-start = ((bf16[16,7,256]{2,1,0:T(8,128)(2,1)}), bf16[16,7,256]{2,1,0:T(8,128)(2,1)S(1)}, u32[]{:S(2)}, u32[]{:S(2)}) async-start(bf16[16,7,256]{2,1,0:T(8,128)(2,1)} %all_to_all.37), calls=%async_computation | async-start | bytes 131072 | tf_op jit(solution)/shard_map/all_to_all | solution.py:97
  47.9 12.8 %copy-start.7 = (bf16[4096]{0:T(1024)(128)(2,1)S(1)}, bf16[4096]{0:T(1024)(128)(2,1)}, u32[]{:S(2)}) copy-start(bf16[4096]{0:T(1024)(128)(2,1)} %param.40) | copy-start | bytes 24580
  47.9 12.8 %copy-start.10 = (s32[7,4]{0,1:T(4,128)S(1)}, s32[7,4]{0,1:T(4,128)}, u32[]{:S(2)}) copy-start(s32[7,4]{0,1:T(4,128)} %param.26) | copy-start | bytes 340
  47.9 13.5 %copy-start.9 = (bf16[2048]{0:T(1024)(128)(2,1)S(1)}, bf16[2048]{0:T(1024)(128)(2,1)}, u32[]{:S(2)}) copy-start(bf16[2048]{0:T(1024)(128)(2,1)} %param.42) | copy-start | bytes 12292
  48.0 13.5 %copy-start.8 = (f32[7,4]{0,1:T(4,128)S(1)}, f32[7,4]{0,1:T(4,128)}, u32[]{:S(2)}) copy-start(f32[7,4]{0,1:T(4,128)} %param.28) | copy-start | bytes 340
  48.0 13.5 %copy-start.12 = (f32[7]{0:T(128)S(1)}, f32[7]{0:T(128)}, u32[]{:S(2)}) copy-start(f32[7]{0:T(128)} %param.27) | copy-start | bytes 88
  48.0 13.5 %copy-start.2 = (bf16[7,2048]{1,0:T(8,128)(2,1)S(1)}, bf16[7,2048]{1,0:T(8,128)(2,1)}, u32[]{:S(2)}) copy-start(bf16[7,2048]{1,0:T(8,128)(2,1)} %param.23) | copy-start | bytes 86020
  48.0 13.5 %copy-start.13 = (bf16[2048,64]{0,1:T(8,128)(2,1)S(1)}, bf16[2048,64]{0,1:T(8,128)(2,1)}, u32[]{:S(2)}) copy-start(bf16[2048,64]{0,1:T(8,128)(2,1)} %param.34) | copy-start | bytes 786436
  48.0 13.5 %copy-start.15 = (f32[64]{0:T(128)S(1)}, f32[64]{0:T(128)}, u32[]{:S(2)}) copy-start(f32[64]{0:T(128)} %param.37) | copy-start | bytes 772
  48.0 20.0 %copy-start.3 = (bf16[7,3,4608]{2,0,1:T(8,128)(2,1)S(1)}, bf16[7,3,4608]{2,0,1:T(8,128)(2,1)}, u32[]{:S(2)}) copy-start(bf16[7,3,4608]{2,0,1:T(8,128)(2,1)} %param.25) | copy-start | bytes 580612
  62.1 12.9 %all-to-all-start.1 = ((bf16[16,7,256]{2,1,0:T(8,128)(2,1)}), bf16[16,7,256]{2,1,0:T(8,128)(2,1)S(1)}, u32[]{:S(2)}, u32[]{:S(2)}) async-start(bf16[16,7,256]{2,1,0:T(8,128)(2,1)} %constant_dynamic-update-slice_fusion), calls=%async_computation.1 | async-start | bytes 131072 | tf_op jit(solution)/shard_map/all_to_all | solution.py:89
  75.5 26.7 %copy-start.1 = (f32[7,4,16,64]{3,2,1,0:T(8,128)}, f32[7,4,16,64]{3,2,1,0:T(8,128)S(1)}, u32[]{:S(2)}) copy-start(f32[7,4,16,64]{3,2,1,0:T(8,128)S(1)} %broadcast_in_dim.7) | copy-start | bytes 344068
  75.5 26.7 %copy-start.11 = (f32[64]{0:T(128)S(1)}, f32[64]{0:T(128)}, u32[]{:S(2)}) copy-start(f32[64]{0:T(128)} %param.39) | copy-start | bytes 772
  127.2 25.1 %all-to-all-start.2 = ((bf16[16,7,128]{2,1,0:T(8,128)(2,1)}), bf16[16,7,128]{2,1,0:T(8,128)(2,1)S(1)}, u32[]{:S(2)}, u32[]{:S(2)}) async-start(bf16[16,7,128]{2,1,0:T(8,128)(2,1)} %all_to_all.42), calls=%async_computation.2 | async-start | bytes 65536 | tf_op jit(solution)/shard_map/all_to_all | solution.py:116
  153.5 16.6 %all-to-all-start.3 = ((bf16[16,3,2048]{2,1,0:T(4,128)(2,1)}), bf16[16,3,2048]{2,1,0:T(4,128)(2,1)S(1)}, u32[]{:S(2)}, u32[]{:S(2)}) async-start(bf16[16,3,2048]{2,1,0:T(4,128)(2,1)} %reshape.111), calls=%async_computation.3 | async-start | bytes 524288 | tf_op jit(solution)/shard_map/all_to_all | solution.py:136
  170.0 11.6 %copy-start.4 = (bf16[7,3,4608]{2,0,1:T(8,128)(2,1)S(1)}, bf16[7,3,4608]{2,0,1:T(8,128)(2,1)}, u32[]{:S(2)}) copy-start(bf16[7,3,4608]{2,0,1:T(8,128)(2,1)} %param.25) | copy-start | bytes 580612
  175.6 16.0 %all-to-all-start.4 = ((bf16[16,3,2048]{2,1,0:T(4,128)(2,1)}), bf16[16,3,2048]{2,1,0:T(4,128)(2,1)S(1)}, u32[]{:S(2)}, u32[]{:S(2)}) async-start(bf16[16,3,2048]{2,1,0:T(4,128)(2,1)} %reshape.113), calls=%async_computation.4 | async-start | bytes 524288 | tf_op jit(solution)/shard_map/all_to_all | solution.py:145
